TPU v7x, 32 devices: a whole 2x2x4 slice. The times are simulated.
32 devices in a mesh: ra: 16 (over z, y, x), cb: 2 (over core).
Axes of the slice: x: 2, y: 2, z: 4, core: 2. Of those that a mesh axis runs over, the one named last changes fastest.
Arguments:
- activations: bfloat16 [768, 4096], P('ra', 'cb'), may hold values from -230 to 230
- gain_first: float32 [4096], P('cb'), may hold values from 0.1 to 1.9
- gate_weight: float32 [11264, 4096], P('ra', 'cb'), may hold values from -0.125 to 0.125
- gate_scale: float32 [11264], P('ra'), may hold values from 0.5 to 2
- up_weight: float32 [11264, 4096], P('ra', 'cb'), may hold values from -0.125 to 0.125
- up_scale: float32 [11264], P('ra'), may hold values from 0.5 to 2
- down_weight: float32 [11264, 4096], P('ra', 'cb'), may hold values from -0.0546875 to 0.0546875
- down_scale: float32 [4096], P('cb'), may hold values from 0.35 to 2.8
- gain_second: float32 [4096], P('cb'), may hold values from 0.1 to 1.9
Outputs:
- normed: bfloat16 [768, 4096], P('ra', 'cb')
All inputs are finite; a program needn't handle non-finite values.
Results may differ from a plain program's by a relative error of at most 0.011.
Values may be sent and summed in bfloat16 or wider, within the bound.
A program may use at most 64 MiB of HBM per device.

v0:
```python
import jax
import jax.numpy as jnp
from jax import lax
from jax.sharding import PartitionSpec as P

EPS = 1e-06


def per_device(
    activations,
    gain_first,
    gate_weight,
    gate_scale,
    up_weight,
    up_scale,
    down_weight,
    down_scale,
    gain_second,
):
    inputs = activations.astype(jnp.float32)
    features = activations.shape[1] * lax.axis_size("cb")
    gate_local = gate_weight.astype(jnp.bfloat16)
    up_local = up_weight.astype(jnp.bfloat16)
    down_local = down_weight.astype(jnp.bfloat16)
    gathered = lax.all_gather(activations, "ra", axis=0, tiled=True)
    wide_rows = gathered.astype(jnp.float32)
    row_squares = jnp.sum(wide_rows * wide_rows, axis=1)
    scaled = (wide_rows * gain_first).astype(jnp.bfloat16)
    contract = (((1,), (1,)), ((), ()))
    squares = lax.psum(row_squares, "cb")
    gate_part = lax.dot_general(gate_local, scaled, contract, preferred_element_type=jnp.float32)
    up_part = lax.dot_general(up_local, scaled, contract, preferred_element_type=jnp.float32)
    gate_sum, up_sum = lax.psum((gate_part, up_part), "cb")
    rscale_first = lax.rsqrt(squares / features + EPS)[None, :]
    gate_full = gate_sum * rscale_first * gate_scale[:, None]
    up_full = up_sum * rscale_first * up_scale[:, None]
    hidden = (jax.nn.silu(gate_full) * up_full).astype(jnp.bfloat16)
    summed = lax.psum_scatter(
        lax.dot_general(
            hidden, down_local, (((0,), (0,)), ((), ())), preferred_element_type=jnp.float32
        ),
        "ra",
        scatter_dimension=0,
        tiled=True,
    )
    stream = 0.1 * inputs + summed * down_scale
    second = lax.psum(jnp.sum(stream * stream, axis=1), "cb")
    rscale_second = lax.rsqrt(second / features + EPS)[:, None]
    return (stream * rscale_second * gain_second).astype(jnp.bfloat16)


def solution(mesh):
    placed = (
        P("ra", "cb"),
        P("cb"),
        P("ra", "cb"),
        P("ra"),
        P("ra", "cb"),
        P("ra"),
        P("ra", "cb"),
        P("cb"),
        P("cb"),
    )
    return jax.shard_map(
        per_device, mesh=mesh, in_specs=placed, out_specs=P("ra", "cb"), check_vma=False
    )
```

profile of v0, /device:TPU:0, one launch (start us, length us, event | category | flops | bytes accessed | tf_op | source)
XLA Modules:
  0.0 292.0 jit_solution(9927717845892913069)
XLA Ops:
  6.5 0.0 all-gather.2.cloned.1.call-start
  6.5 0.7 all-gather.2.cloned.1.call-update
  7.3 0.0 copy-start.4
  7.3 0.0 all-reduce.3.cloned.1.call-start
  7.3 73.4 %all-gather.2.cloned.1.call-done = bf16[768,2048]{1,0:T(8,128)(2,1)} async-done(((bf16[48,2048]{1,0:T(8,128)(2,1)}), bf16[768,2048]{1,0:T(8,128)(2,1)}) %all-gather.2.cloned.1.call-update) | async-done | bytes 3145744 | tf_op jit(solution)/shard_map/all_gather | solution.py:25
  80.7 0.0 copy-start
  80.7 7.5 %fusion.15 = f32[704,768]{1,0:T(8,128)} fusion(f32[704,2048]{1,0:T(8,128)} %param.13, bf16[768,2048]{1,0:T(8,128)(2,1)} %all-gather.2.cloned.1.call-done, f32[2048]{0:T(1024)} %param.10), kind=kOutput, calls=%fused_computation.12 | convolution fusion | flops 2220752896 | bytes 11083776 | tf_op jit(solution)/shard_map/dot_general | solution.py:32
  88.3 0.0 copy-done.4
  88.3 0.0 copy-done
  88.3 6.4 %fusion.10 = f32[704,768]{1,0:T(8,128)} fusion(f32[704,2048]{1,0:T(8,128)} %param.11, bf16[768,2048]{1,0:T(8,128)(2,1)S(1)} %copy-done, f32[2048]{0:T(1024)S(1)} %copy-done.4), kind=kOutput, calls=%fused_computation.11 | convolution fusion | flops 2220752896 | bytes 11083776 | tf_op jit(solution)/shard_map/dot_general | solution.py:31
  94.7 0.0 copy-start.5
  94.7 0.0 copy-start.6
  94.7 0.0 all-reduce.3.cloned.1.call-update
  94.7 0.0 reduce-scatter.2.cloned.1.call-start
  94.8 0.7 fusion.1
  95.5 2.5 psum.29
  97.9 23.9 %all-reduce.3.cloned.1.call-done = (f32[704,768]{1,0:T(8,128)}, f32[704,768]{1,0:T(8,128)}) async-done(((f32[704,768]{1,0:T(8,128)}, f32[704,768]{1,0:T(8,128)}), (f32[704,768]{1,0:T(8,128)}, f32[704,768]{1,0:T(8,128)})) %all-reduce.3.cloned.1.call-update) | async-done | bytes 4325392 | tf_op jit(solution)/shard_map/psum | solution.py:33
  121.9 0.0 copy-done.5
  121.9 0.0 copy-done.6
  121.9 9.5 %fusion.2 = f32[768,2048]{1,0:T(8,128)} fusion(f32[704,2048]{1,0:T(8,128)} %param.15, f32[704,768]{1,0:T(8,128)} %get-tuple-element.5, f32[704,768]{1,0:T(8,128)} %get-tuple-element.6, f32[704]{0:T(1024)S(1)} %copy-done.5, f32[704]{0:T(1024)S(1)} %copy-done.6, f32[768]{0:T(1024)S(1)} %add_rsqrt_fusion), kind=kOutput, calls=%fused_computation.4 | convolution fusion | flops 2221441024 | bytes 16392704 | tf_op jit(solution)/shard_map/dot_general | solution.py:39
  131.3 0.0 copy-start.1
  131.3 0.0 copy-start.2
  131.4 0.0 copy-start.3
  131.4 0.0 reduce-scatter.2.cloned.1.call-update
  131.4 148.7 %reduce-scatter.2.cloned.1.call-done = f32[48,2048]{1,0:T(8,128)} async-done(((f32[768,2048]{1,0:T(8,128)}), f32[48,2048]{1,0:T(8,128)}) %reduce-scatter.2.cloned.1.call-update) | async-done | bytes 393232 | tf_op jit(solution)/shard_map/reduce_scatter | solution.py:38
  280.1 0.0 copy-done.1
  280.1 0.0 copy-done.2
  280.1 1.2 multiply_reduce_fusion
  281.2 2.5 psum.31
  283.7 0.0 copy-done.3
  283.7 1.8 multiply_convert_fusion.2
  (2 shorter events, 0.0 us)
Async XLA Ops:
  6.5 74.2 %all-gather.2.cloned.1.call-start = ((), (), s32[]{:S(2)}) async-start(), calls=%async_computation.1 | async-start | bytes 3342336 | tf_op jit(solution)/shard_map/all_gather | solution.py:25
  7.3 81.0 %copy-start.4 = (f32[2048]{0:T(1024)S(1)}, f32[2048]{0:T(1024)}, u32[]{:S(2)}) copy-start(f32[2048]{0:T(1024)} %param.10) | copy-start | bytes 24580
  7.3 114.6 %all-reduce.3.cloned.1.call-start = ((), (), s32[]{:S(2)}) async-start(), calls=%async_computation.3 | async-start | bytes 8650752 | tf_op jit(solution)/shard_map/psum | solution.py:33
  80.7 7.6 %copy-start = (bf16[768,2048]{1,0:T(8,128)(2,1)S(1)}, bf16[768,2048]{1,0:T(8,128)(2,1)}, u32[]{:S(2)}) copy-start(bf16[768,2048]{1,0:T(8,128)(2,1)} %all-gather.2.cloned.1.call-done) | copy-start | bytes 9437188
  94.7 27.2 %copy-start.5 = (f32[704]{0:T(1024)S(1)}, f32[704]{0:T(1024)}, u32[]{:S(2)}) copy-start(f32[704]{0:T(1024)} %param.14) | copy-start | bytes 8452
  94.7 27.2 %copy-start.6 = (f32[704]{0:T(1024)S(1)}, f32[704]{0:T(1024)}, u32[]{:S(2)}) copy-start(f32[704]{0:T(1024)} %param.12) | copy-start | bytes 8452
  94.7 185.3 %reduce-scatter.2.cloned.1.call-start = ((), (), s32[]{:S(2)}) async-start(), calls=%async_computation.2 | async-start | bytes 6684672 | tf_op jit(solution)/shard_map/reduce_scatter | solution.py:38
  131.3 148.7 %copy-start.1 = (bf16[48,2048]{1,0:T(8,128)(2,1)S(1)}, bf16[48,2048]{1,0:T(8,128)(2,1)}, u32[]{:S(2)}) copy-start(bf16[48,2048]{1,0:T(8,128)(2,1)} %param.9) | copy-start | bytes 589828
  131.3 148.7 %copy-start.2 = (f32[2048]{0:T(1024)S(1)}, f32[2048]{0:T(1024)}, u32[]{:S(2)}) copy-start(f32[2048]{0:T(1024)} %param.16) | copy-start | bytes 24580
  131.4 152.4 %copy-start.3 = (f32[2048]{0:T(1024)S(1)}, f32[2048]{0:T(1024)}, u32[]{:S(2)}) copy-start(f32[2048]{0:T(1024)} %param.17) | copy-start | bytes 24580
Sparse Core Ops, SparseCore 0:
  10.1 70.5 all-gather.1
  94.9 26.9 all-reduce.2
  131.5 148.5 reduce-scatter.1
where the time goes:
time: 292 us
  waiting for transfers between devices  247 us (85%)
  matrix products  23.4 us (8%)
  between operations  13.1 us (4%)
  blocking collectives  4.95 us (2%)
  other arithmetic  3.66 us (1%)
    reduce_scatter x1, waiting for transfers between devices, per_device(): lax.psum_scatter(lax.dot_general(hidden, down_local, (((0,), (0,)), ((),...  149 us
    all_gather x1, waiting for transfers between devices, per_device(): gathered = lax.all_gather(activations, 'ra', axis=0, tiled=True)  73.4 us
    psum x1, waiting for transfers between devices, per_device(): gate_sum, up_sum = lax.psum((gate_part, up_part), 'cb')  23.9 us
    dot_general x1, matrix products, per_device(): lax.dot_general(hidden, down_local, (((0,), (0,)), ((), ())), preferred_e...  9.48 us
    dot_general x1, matrix products, per_device(): lax.dot_general(up_local, scaled, contract, preferred_element_type=jnp.fl...  7.55 us
    dot_general x1, matrix products, per_device(): lax.dot_general(gate_local, scaled, contract, preferred_element_type=jnp....  6.42 us
  transfers between devices with their start and end apart: 3, of which 3 were waited for; matrix products, arithmetic and copies ran while one was open for 0% of the time, Pallas kernels for 0%

commit v1 on v0

v1 whole, which is shorter than its diff:
```python
import functools

import jax
import jax.numpy as jnp
from jax import lax
from jax.experimental import pallas as pl
from jax.experimental.pallas import tpu as pltpu
from jax.sharding import PartitionSpec as P

EPS = 1e-06
MESH = pl.DeviceIdType.MESH
F32 = jnp.float32
BF16 = jnp.bfloat16


def flip(index, mask):
    bit = 1
    while bit <= mask:
        if mask & bit:
            index = index + (1 - 2 * ((index // bit) % 2)) * bit
        bit *= 2
    return index


def kernel(
    planes,
    features,
    x_ref,
    gain_ref,
    gate_hbm,
    gate_scale_ref,
    up_hbm,
    up_scale_ref,
    down_hbm,
    down_scale_ref,
    gain2_ref,
    out_ref,
    wide,
    gate_w,
    up_w,
    down_w,
    xg,
    scaled,
    hidden,
    part,
    ex_send,
    ex_recv,
    sq_send,
    sq_recv,
    keep_a,
    keep_b,
    send_a,
    send_b,
    recv_a,
    recv_b,
    send2_a,
    send2_b,
    recv2_a,
    recv2_b,
    own_sum,
    z_send,
    z_recv,
    last_send,
    last_recv,
    w_sem,
    ssem,
    rsem,
):
    ra = lax.axis_index("ra")
    cb = lax.axis_index("cb")
    rows, width = x_ref.shape
    half = width // 2
    x_peer = (flip(ra, 1), cb)
    y_peer = (flip(ra, 2), cb)
    z_peers = [None] + [(flip(ra, 4 * k), cb) for k in range(1, planes)]
    core_peer = (ra, flip(cb, 1))
    first, second = pl.ds(0, half), pl.ds(half, half)

    loads = []
    for i, src in enumerate((gate_hbm, up_hbm, down_hbm)):
        load = pltpu.make_async_copy(src, wide.at[i], w_sem.at[i])
        load.start()
        loads.append(load)

    barrier = pltpu.get_barrier_semaphore()
    peers = [x_peer, y_peer, core_peer] + z_peers[1:]
    for peer in peers:
        pl.semaphore_signal(barrier, inc=1, device_id=peer, device_id_type=MESH)
    pl.semaphore_wait(barrier, len(peers))

    copies = {}

    def send(name, k, src, dst, peer):
        slot = len(copies)
        copy = pltpu.make_async_remote_copy(
            src_ref=src,
            dst_ref=dst,
            send_sem=ssem.at[slot],
            recv_sem=rsem.at[slot],
            device_id=peer,
            device_id_type=MESH,
        )
        copy.start()
        copies[name, k] = copy

    def arrived(name, k):
        copies[name, k].wait_recv()

    def spread(k):
        src = x_ref if k == 0 else xg.at[k, 0]
        if k:
            arrived("z", k)
        send("gx", k, src, xg.at[k, 1], x_peer)
        send("gy", k, src, xg.at[k, 2], y_peer)

    def forward(k):
        arrived("gx", k)
        send("fy", k, xg.at[k, 1, :, second], xg.at[k, 3, :, second], y_peer)
        arrived("gy", k)
        send("fx", k, xg.at[k, 2, :, first], xg.at[k, 3, :, first], x_peer)

    nt = (((1,), (1,)), ((), ()))

    def gate_up(k):
        arrived("fx", k)
        arrived("fy", k)

        def prepare(s, carry):
            block = xg[k, s].astype(F32)
            squares = jnp.sum(block * block, axis=1, keepdims=True)
            sq_send[k, s] = jnp.broadcast_to(squares, (rows, 128))
            scaled[s] = (block * gain_ref[...]).astype(BF16)
            return carry

        lax.fori_loop(0, 4, prepare, 0)
        send("sq", k, sq_send.at[k], sq_recv.at[k], core_peer)
        tokens = scaled[...].reshape(4 * rows, width)
        for i, w in enumerate((gate_w, up_w)):
            product = lax.dot_general(tokens, w[...], nt, preferred_element_type=F32)
            part[k, i] = product
            ex_send[k, i] = product.astype(BF16)
            send(("ex", i), k, ex_send.at[k, i], ex_recv.at[k, i], core_peer)

    def down(k):
        arrived("sq", k)
        arrived(("ex", 0), k)
        arrived(("ex", 1), k)

        for s in range(4):
            here = slice(s * rows, (s + 1) * rows)
            squares = (sq_send[k, s] + sq_recv[k, s])[:, :1]
            rscale = lax.rsqrt(squares / features + EPS)
            gate = (part[k, 0, here] + ex_recv[k, 0, here].astype(F32)) * rscale * gate_scale_ref[...]
            up = (part[k, 1, here] + ex_recv[k, 1, here].astype(F32)) * rscale * up_scale_ref[...]
            hidden[here] = (gate / (1.0 + jnp.exp(-gate)) * up).astype(BF16)
        units = hidden[...]
        prod = jnp.dot(units, down_w[:, :half], preferred_element_type=F32)
        for dy in range(2):
            low = 2 * dy * rows
            keep_a[k, dy] = prod[low : low + rows]
            send_a[k, dy] = prod[low + rows : low + 2 * rows].astype(BF16)
        send("a1", k, send_a.at[k], recv_a.at[k], x_peer)
        prod = jnp.dot(units, down_w[:, half:], preferred_element_type=F32)
        for dx in range(2):
            low = dx * rows
            keep_b[k, dx] = prod[low : low + rows]
            low += 2 * rows
            send_b[k, dx] = prod[low : low + rows].astype(BF16)
        send("b1", k, send_b.at[k], recv_b.at[k], y_peer)

    def reduce_one(k):
        arrived("a1", k)
        send2_a[k] = (keep_a[k, 1] + recv_a[k, 1].astype(F32)).astype(BF16)
        send("a2", k, send2_a.at[k], recv2_a.at[k], y_peer)
        arrived("b1", k)
        send2_b[k] = (keep_b[k, 1] + recv_b[k, 1].astype(F32)).astype(BF16)
        send("b2", k, send2_b.at[k], recv2_b.at[k], x_peer)

    def reduce_two(k):
        arrived("a2", k)
        sum_a = keep_a[k, 0] + recv_a[k, 0].astype(F32) + recv2_a[k].astype(F32)
        arrived("b2", k)
        sum_b = keep_b[k, 0] + recv_b[k, 0].astype(F32) + recv2_b[k].astype(F32)
        if k == 0:
            own_sum[:, :half] = sum_a
            own_sum[:, half:] = sum_b
        else:
            z_send[k, :, :half] = sum_a.astype(BF16)
            z_send[k, :, half:] = sum_b.astype(BF16)
            send("zs", k, z_send.at[k], z_recv.at[k], z_peers[k])

    def narrow(i, target):
        loads[i].wait()
        step = 64

        def body(j, carry):
            here = pl.ds(pl.multiple_of(j * step, step), step)
            target[here] = wide[i, here].astype(BF16)
            return carry

        lax.fori_loop(0, target.shape[0] // step, body, 0)

    spread(0)
    for k in range(1, planes):
        send("z", k, x_ref, xg.at[k, 0], z_peers[k])
    xg[0, 0] = x_ref[...]
    narrow(0, gate_w)
    forward(0)
    spread(1)
    narrow(1, up_w)
    gate_up(0)
    narrow(2, down_w)
    order = list(range(1, planes))
    for k in order:
        forward(k)
        if k + 1 < planes:
            spread(k + 1)
        if k > 1:
            down(k - 1)
        gate_up(k)
    down(planes - 1)
    late = order + [0]
    reduce_one(1)
    down(0)
    for at in range(1, planes):
        reduce_one(late[at])
        reduce_two(late[at - 1])
    reduce_two(0)

    total = own_sum[...]
    for k in range(1, planes):
        arrived("zs", k)
        total = total + z_recv[k].astype(F32)
    stream = 0.1 * x_ref[...].astype(F32) + total * down_scale_ref[...]
    own_sum[...] = stream
    last_send[...] = jnp.broadcast_to(
        jnp.sum(stream * stream, axis=1, keepdims=True), last_send.shape
    )
    send("last", 0, last_send, last_recv, core_peer)
    arrived("last", 0)
    both = (last_send[...] + last_recv[...])[:, :1]
    rscale = lax.rsqrt(both / features + EPS)
    out_ref[...] = (own_sum[...] * rscale * gain2_ref[...]).astype(BF16)
    for copy in copies.values():
        copy.wait_send()


def fused(
    planes,
    activations,
    gain_first,
    gate_weight,
    gate_scale,
    up_weight,
    up_scale,
    down_weight,
    down_scale,
    gain_second,
):
    rows, width = activations.shape
    units = gate_weight.shape[0]
    half = width // 2
    group = 4 * rows
    n_copies = 16 * planes
    vmem = pl.BlockSpec(memory_space=pltpu.VMEM)
    hbm = pl.BlockSpec(memory_space=pl.ANY)
    scratch = [
        pltpu.VMEM((3, units, width), F32),
        pltpu.VMEM((units, width), BF16),
        pltpu.VMEM((units, width), BF16),
        pltpu.VMEM((units, width), BF16),
        pltpu.VMEM((planes, 4, rows, width), BF16),
        pltpu.VMEM((4, rows, width), BF16),
        pltpu.VMEM((group, units), BF16),
        pltpu.VMEM((planes, 2, group, units), F32),
        pltpu.VMEM((planes, 2, group, units), BF16),
        pltpu.VMEM((planes, 2, group, units), BF16),
        pltpu.VMEM((planes, 4, rows, 128), F32),
        pltpu.VMEM((planes, 4, rows, 128), F32),
        pltpu.VMEM((planes, 2, rows, half), F32),
        pltpu.VMEM((planes, 2, rows, half), F32),
        pltpu.VMEM((planes, 2, rows, half), BF16),
        pltpu.VMEM((planes, 2, rows, half), BF16),
        pltpu.VMEM((planes, 2, rows, half), BF16),
        pltpu.VMEM((planes, 2, rows, half), BF16),
        pltpu.VMEM((planes, rows, half), BF16),
        pltpu.VMEM((planes, rows, half), BF16),
        pltpu.VMEM((planes, rows, half), BF16),
        pltpu.VMEM((planes, rows, half), BF16),
        pltpu.VMEM((rows, width), F32),
        pltpu.VMEM((planes, rows, width), BF16),
        pltpu.VMEM((planes, rows, width), BF16),
        pltpu.VMEM((rows, 128), F32),
        pltpu.VMEM((rows, 128), F32),
        pltpu.SemaphoreType.DMA((3,)),
        pltpu.SemaphoreType.DMA((n_copies,)),
        pltpu.SemaphoreType.DMA((n_copies,)),
    ]
    return pl.pallas_call(
        functools.partial(kernel, planes, width * 2),
        out_shape=jax.ShapeDtypeStruct((rows, width), BF16),
        in_specs=[vmem, vmem, hbm, vmem, hbm, vmem, hbm, vmem, vmem],
        out_specs=vmem,
        scratch_shapes=scratch,
        compiler_params=pltpu.CompilerParams(
            collective_id=0, has_side_effects=True, vmem_limit_bytes=60 * 1024 * 1024
        ),
    )(
        activations,
        gain_first[None, :],
        gate_weight,
        gate_scale[None, :],
        up_weight,
        up_scale[None, :],
        down_weight,
        down_scale[None, :],
        gain_second[None, :],
    )


def plain(
    activations,
    gain_first,
    gate_weight,
    gate_scale,
    up_weight,
    up_scale,
    down_weight,
    down_scale,
    gain_second,
):
    inputs = activations.astype(F32)
    features = activations.shape[1] * lax.axis_size("cb")
    gate_local = gate_weight.astype(BF16)
    up_local = up_weight.astype(BF16)
    down_local = down_weight.astype(BF16)
    gathered = lax.all_gather(activations, "ra", axis=0, tiled=True)
    wide_rows = gathered.astype(F32)
    row_squares = jnp.sum(wide_rows * wide_rows, axis=1)
    scaled = (wide_rows * gain_first).astype(BF16)
    contract = (((1,), (1,)), ((), ()))
    squares = lax.psum(row_squares, "cb")
    gate_part = lax.dot_general(gate_local, scaled, contract, preferred_element_type=F32)
    up_part = lax.dot_general(up_local, scaled, contract, preferred_element_type=F32)
    gate_sum, up_sum = lax.psum((gate_part, up_part), "cb")
    rscale_first = lax.rsqrt(squares / features + EPS)[None, :]
    gate_full = gate_sum * rscale_first * gate_scale[:, None]
    up_full = up_sum * rscale_first * up_scale[:, None]
    hidden = (jax.nn.silu(gate_full) * up_full).astype(BF16)
    mixed = lax.dot_general(hidden, down_local, (((0,), (0,)), ((), ())), preferred_element_type=F32)
    summed = lax.psum_scatter(mixed, "ra", scatter_dimension=0, tiled=True)
    stream = 0.1 * inputs + summed * down_scale
    second = lax.psum(jnp.sum(stream * stream, axis=1), "cb")
    rscale_second = lax.rsqrt(second / features + EPS)[:, None]
    return (stream * rscale_second * gain_second).astype(BF16)


def solution(mesh):
    placed = (
        P("ra", "cb"),
        P("cb"),
        P("ra", "cb"),
        P("ra"),
        P("ra", "cb"),
        P("ra"),
        P("ra", "cb"),
        P("cb"),
        P("cb"),
    )
    planes = mesh.shape["ra"] // 4
    paired = mesh.shape["cb"] == 2 and planes >= 2 and planes & (planes - 1) == 0
    body = functools.partial(fused, planes) if paired else plain
    return jax.shard_map(
        body, mesh=mesh, in_specs=placed, out_specs=P("ra", "cb"), check_vma=False
    )
```

time: 292 us -> 82.8 us (0.28)
  waiting for transfers between devices: 247 us -> 0 us
  Pallas kernels: 0 us -> 77.4 us
  matrix products: 23.4 us -> 0 us
  between operations: 13.1 us -> 0.01 us
  blocking collectives: 4.95 us -> 0 us
  local copies, waits for them, and re-layouts: 0.03 us -> 4.15 us
  other arithmetic: 3.66 us -> 0 us
    reduce_scatter x1 -> x0, waiting for transfers between devices: 149 us -> none  [per_device(): lax.psum_scatter(lax.dot_general(hidden, down_local, (((0,), (0,)), ((),...]
    pallas_call x0 -> x1, Pallas kernels: none -> 77.4 us  [fused(): pl.pallas_call(functools.partial(kernel, planes, width * 2), out_shape=ja...]
    all_gather x1 -> x0, waiting for transfers between devices: 73.4 us -> none  [per_device(): gathered = lax.all_gather(activations, 'ra', axis=0, tiled=True)]
    psum x1 -> x0, waiting for transfers between devices: 23.9 us -> none  [per_device(): gate_sum, up_sum = lax.psum((gate_part, up_part), 'cb')]
    dot_general x3 -> x0, matrix products: 23.4 us -> none  [the longest x1 9.48 us: per_device(): lax.dot_general(hidden, down_local, (((0,), (0,)), ((), ())), preferred_e...]
    psum x2 -> x0, blocking collectives: 4.95 us -> none  [the longest x1 2.47 us: per_device(): squares = lax.psum(row_squares, 'cb')]
  transfers between devices with their start and end apart: 3 -> 0, of which waited for: 3 -> 0; matrix products, arithmetic and copies ran while one was open for 0% -> 0% of each run, Pallas kernels for 0% -> 0%
where the time goes in v1:
time: 82.8 us; the launch traced here: 81.6 us
  Pallas kernels  77.4 us (93%)
  local copies, waits for them, and re-layouts  4.15 us (5%)
    pallas_call x1, Pallas kernels, fused(): pl.pallas_call(functools.partial(kernel, planes, width * 2), out_shape=ja...  77.4 us

profile of v1, /device:TPU:0, one launch (start us, length us, event | category | flops | bytes accessed | tf_op | source)
XLA Modules:
  0.0 81.6 jit_solution(7904344601056640600)
XLA Ops:
  0.0 1.3 %broadcast_in_dim.16.gate_scale_ref = f32[1,704]{1,0:T(1,128)} reshape(f32[704]{0:T(1024)} %param.12) | data formatting | bytes 5632 | tf_op jit(solution)/shard_map/broadcast_in_dim | solution.py:312
  1.3 1.3 %broadcast_in_dim.17.up_scale_ref = f32[1,704]{1,0:T(1,128)} reshape(f32[704]{0:T(1024)} %param.14) | data formatting | bytes 5632 | tf_op jit(solution)/shard_map/broadcast_in_dim | solution.py:314
  2.5 77.4 %shard_map.91 = bf16[48,2048]{1,0:T(8,128)(2,1)} custom-call(bf16[48,2048]{1,0:T(8,128)(2,1)} %x_ref.1, f32[1,2048]{1,0:T(1,128)} %bitcast.3, f32[704,2048]{1,0:T(8,128)} %gate_hbm.1, f32[1,704]{1,0:T(1,128)} %broadcast_in_dim.16.gate_scale_ref, f32[704,2048]{1,0:T(8,128)} %up_hbm.1, f32[1,704]{1,0:T(1,128)} %broadcast_in_dim.17.up_scale_ref, ...), custom_call_target="tpu_custom_call" | custom-call | tf_op jit(solution)/shard_map/pallas_call | solution.py:299
  79.9 1.6 %copy.11 = bf16[48,2048]{1,0:T(8,128)(2,1)} copy(bf16[48,2048]{1,0:T(8,128)(2,1)} %shard_map.91) | data formatting | bytes 393216

commit v2 on v1

--- a/solution.py
+++ b/solution.py
@@ -106,22 +106,28 @@
     def arrived(name, k):
         copies[name, k].wait_recv()
 
+    halves = (first, second)
+
     def spread(k):
-        src = x_ref if k == 0 else xg.at[k, 0]
-        if k:
-            arrived("z", k)
-        send("gx", k, src, xg.at[k, 1], x_peer)
-        send("gy", k, src, xg.at[k, 2], y_peer)
+        for i in (1, 0):
+            if k:
+                arrived(("z", i), k)
+            for name, slot, peer in (("gx", 1, x_peer), ("gy", 2, y_peer)):
+                h = i if k or name == "gx" else 1 - i
+                src = (xg.at[k, 0] if k else x_ref).at[:, halves[h]]
+                send((name, h), k, src, xg.at[k, slot, :, halves[h]], peer)
 
     def forward(k):
-        arrived("gx", k)
+        arrived(("gx", 1), k)
         send("fy", k, xg.at[k, 1, :, second], xg.at[k, 3, :, second], y_peer)
-        arrived("gy", k)
+        arrived(("gy", 0), k)
         send("fx", k, xg.at[k, 2, :, first], xg.at[k, 3, :, first], x_peer)
 
     nt = (((1,), (1,)), ((), ()))
 
     def gate_up(k):
+        arrived(("gx", 0), k)
+        arrived(("gy", 1), k)
         arrived("fx", k)
         arrived("fy", k)
 
@@ -150,8 +156,8 @@
             here = slice(s * rows, (s + 1) * rows)
             squares = (sq_send[k, s] + sq_recv[k, s])[:, :1]
             rscale = lax.rsqrt(squares / features + EPS)
-            gate = (part[k, 0, here] + ex_recv[k, 0, here].astype(F32)) * rscale * gate_scale_ref[...]
-            up = (part[k, 1, here] + ex_recv[k, 1, here].astype(F32)) * rscale * up_scale_ref[...]
+            gate = (part[k, 0, here] + ex_recv[k, 0, here].astype(F32)) * rscale * gate_scale_ref[...][None, :]
+            up = (part[k, 1, here] + ex_recv[k, 1, here].astype(F32)) * rscale * up_scale_ref[...][None, :]
             hidden[here] = (gate / (1.0 + jnp.exp(-gate)) * up).astype(BF16)
         units = hidden[...]
         prod = jnp.dot(units, down_w[:, :half], preferred_element_type=F32)
@@ -159,13 +165,15 @@
             low = 2 * dy * rows
             keep_a[k, dy] = prod[low : low + rows]
             send_a[k, dy] = prod[low + rows : low + 2 * rows].astype(BF16)
-        send("a1", k, send_a.at[k], recv_a.at[k], x_peer)
         prod = jnp.dot(units, down_w[:, half:], preferred_element_type=F32)
         for dx in range(2):
             low = dx * rows
             keep_b[k, dx] = prod[low : low + rows]
             low += 2 * rows
             send_b[k, dx] = prod[low : low + rows].astype(BF16)
+
+    def issue(k):
+        send("a1", k, send_a.at[k], recv_a.at[k], x_peer)
         send("b1", k, send_b.at[k], recv_b.at[k], y_peer)
 
     def reduce_one(k):
@@ -202,26 +210,39 @@
 
     spread(0)
     for k in range(1, planes):
-        send("z", k, x_ref, xg.at[k, 0], z_peers[k])
+        for i in (1, 0):
+            part_of = pl.ds(i * half, half)
+            send(("z", i), k, x_ref.at[:, part_of], xg.at[k, 0, :, part_of], z_peers[k])
     xg[0, 0] = x_ref[...]
-    narrow(0, gate_w)
     forward(0)
     spread(1)
+    narrow(0, gate_w)
     narrow(1, up_w)
     gate_up(0)
-    narrow(2, down_w)
-    order = list(range(1, planes))
-    for k in order:
-        forward(k)
+    forward(1)
+    for k in range(1, planes):
         if k + 1 < planes:
             spread(k + 1)
-        if k > 1:
+        if k == 1:
+            narrow(2, down_w)
+        if k > 2:
             down(k - 1)
+            issue(k - 1)
+        elif k == 2:
+            down(1)
+            issue(1)
         gate_up(k)
+        if k + 1 < planes:
+            forward(k + 1)
+    late = list(range(1, planes)) + [0]
+    down(0)
+    if planes > 2:
+        reduce_one(1)
     down(planes - 1)
-    late = order + [0]
-    reduce_one(1)
-    down(0)
+    issue(planes - 1)
+    issue(0)
+    if planes == 2:
+        reduce_one(1)
     for at in range(1, planes):
         reduce_one(late[at])
         reduce_two(late[at - 1])
@@ -261,7 +282,7 @@
     units = gate_weight.shape[0]
     half = width // 2
     group = 4 * rows
-    n_copies = 16 * planes
+    n_copies = 20 * planes
     vmem = pl.BlockSpec(memory_space=pltpu.VMEM)
     hbm = pl.BlockSpec(memory_space=pl.ANY)
     scratch = [
@@ -309,9 +330,9 @@
         activations,
         gain_first[None, :],
         gate_weight,
-        gate_scale[None, :],
+        gate_scale,
         up_weight,
-        up_scale[None, :],
+        up_scale,
         down_weight,
         down_scale[None, :],
         gain_second[None, :],

time: 82.8 us -> 80.1 us (0.967)
  local copies, waits for them, and re-layouts: 4.15 us -> 1.62 us
    broadcast_in_dim x2 -> x0, local copies, waits for them, and re-layouts: 2.53 us -> none  [the longest x1 1.27 us: fused(): gate_scale[None, :]]
where the time goes in v2:
time: 80.1 us; the launch traced here: 78.5 us
  Pallas kernels  76.9 us (96%)
  local copies, waits for them, and re-layouts  1.62 us (2%)
    pallas_call x1, Pallas kernels, fused(): pl.pallas_call(functools.partial(kernel, planes, width * 2), out_shape=ja...  76.9 us
    unnamed x1, local copies, waits for them, and re-layouts  1.62 us

profile of v2, /device:TPU:0, one launch (start us, length us, event | category | flops | bytes accessed | tf_op | source)
XLA Modules:
  0.0 78.5 jit_solution(5321093766934675064)
XLA Ops:
  0.0 76.9 %shard_map.91 = bf16[48,2048]{1,0:T(8,128)(2,1)} custom-call(bf16[48,2048]{1,0:T(8,128)(2,1)} %x_ref.1, f32[1,2048]{1,0:T(1,128)} %bitcast.3, f32[704,2048]{1,0:T(8,128)} %gate_hbm.1, f32[704]{0:T(1024)} %gate_scale_ref.1, f32[704,2048]{1,0:T(8,128)} %up_hbm.1, f32[704]{0:T(1024)} %up_scale_ref.1, f32[704,2048]{1,0:T(8,128)} %down_hbm.1, f32[1,2048]{1,0:T(1,128)} %bitcast.4, ...), custom_call_target="tpu_custom_call" | custom-call | tf_op jit(solution)/shard_map/pallas_call | solution.py:320
  76.9 1.6 %copy.11 = bf16[48,2048]{1,0:T(8,128)(2,1)} copy(bf16[48,2048]{1,0:T(8,128)(2,1)} %shard_map.91) | data formatting | bytes 393216
